TPU v7x, 32 devices: a whole 2x2x4 slice. The times are simulated.
32 devices in a mesh: sp: 8 (over z, x), tp: 4 (over y, core).
Axes of the slice: x: 2, y: 2, z: 4, core: 2. Of those that a mesh axis runs over, the one named last changes fastest.
Arguments:
- residual: bfloat16 [2048, 2048], P(('sp', 'tp')), may hold values from -6 to 6
- query_wide: bfloat16 [2048, 512], P('sp', 'tp'), may hold values from -8 to 8
- key_wide: bfloat16 [2048, 512], P('sp', 'tp'), may hold values from -8 to 8
- value_wide: bfloat16 [2048, 512], P('sp', 'tp'), may hold values from -6 to 6
- query_narrow: bfloat16 [2048, 512], P('sp', 'tp'), may hold values from -8 to 8
- key_narrow: bfloat16 [2048, 512], P('sp', 'tp'), may hold values from -8 to 8
- value_narrow: bfloat16 [2048, 512], P('sp', 'tp'), may hold values from -6 to 6
- gate_wide: float32 [2048, 4], P('sp', 'tp'), may hold values from -2 to 20
- gate_narrow: float32 [2048, 8], P('sp', 'tp'), may hold values from -2 to 20
- out_wide: bfloat16 [512, 2048], replicated, may hold values from -0.1875 to 0.1875
- out_narrow: bfloat16 [512, 2048], replicated, may hold values from -0.1875 to 0.1875
- norm_gain: float32 [2048], replicated, may hold values from 0.1 to 1.9
- routing: int32 [2048, 2], P(('sp', 'tp')), may hold values from 0 to 7, as said below
- route_weight: float32 [2048, 2], P(('sp', 'tp')), may hold values from 0.3 to 1.5
- gate_weight: bfloat16 [8, 2048, 1024], P('sp', None, 'tp'), may hold values from -0.125 to 0.125
- up_weight: bfloat16 [8, 2048, 1024], P('sp', None, 'tp'), may hold values from -0.125 to 0.125
- down_weight: bfloat16 [8, 1024, 2048], P('sp', 'tp'), may hold values from -0.1875 to 0.1875
Outputs:
- result: bfloat16 [2048, 2048], P(('sp', 'tp'))
Inputs may be any that keep to these rules, and one draw needn't show every extreme that they name: `routing`: each row names 2 different experts of one group (experts g * 2 to g * 2 + 1). In each aligned block of 64 rows (the rows of one device) no expert is named by more than 32 rows; one group, the same for all blocks, has each of its experts named by exactly 32 rows of every block.
All inputs are finite; a program needn't handle non-finite values.
Results may differ from a plain program's by a relative error of at most 0.017.
Values may be sent and summed in bfloat16 or wider, within the bound.
A program may use at most 128 MiB of HBM per device.

v0:
```python
import math
import jax
import jax.numpy as jnp
from jax import lax
from jax.sharding import PartitionSpec as P

HW = 128
HN = 64
GROUPS = 4
epsilon = 1e-06


def globalize(pieces, shard_rows):
    shards = pieces.shape[0] // shard_rows
    grid = pieces.reshape(shards, shard_rows, pieces.shape[1])
    endings = grid[:, -1, :]
    offsets = jnp.cumsum(endings, axis=0) - endings
    return (grid + offsets[:, None, :]).reshape(pieces.shape)


def head_block(
    state, queries, query_decay, keys, values, key_decay, first_key, first_query, head_width
):
    highest_old, weight_sum, weighted = state
    query_rows = queries.shape[0]
    head_count = query_decay.shape[1]
    key_rows = keys.shape[0]
    grid_query = queries.reshape(query_rows, head_count, head_width)
    grid_key = keys.reshape(key_rows, head_count, head_width)
    grid_value = values.reshape(key_rows, head_count, head_width)
    scores = jnp.einsum("thd,phd->htp", grid_query, grid_key, preferred_element_type=jnp.float32)
    scores = scores * head_width ** (-0.5) + query_decay.T[:, :, None] - key_decay.T[:, None, :]
    query_place = first_query + jnp.arange(query_rows, dtype=jnp.int32)
    key_place = first_key + jnp.arange(key_rows, dtype=jnp.int32)
    scores = jnp.where(key_place[None, None, :] <= query_place[None, :, None], scores, -jnp.inf)
    highest = jnp.maximum(highest_old, jnp.max(scores, axis=2))
    weights = jnp.exp(scores - highest[:, :, None])
    shrink = jnp.exp(highest_old - highest)
    weight_sum = weight_sum * shrink + jnp.sum(weights, axis=2)
    product = jnp.einsum(
        "htp,phd->htd", weights.astype(jnp.bfloat16), grid_value, preferred_element_type=jnp.float32
    )
    weighted = weighted * shrink[:, :, None] + product
    return (highest, weight_sum, weighted)


def fresh_state(head_count, shard_rows, head_width):
    return (
        jnp.full((head_count, shard_rows), -1e30, jnp.float32),
        jnp.zeros((head_count, shard_rows), jnp.float32),
        jnp.zeros((head_count, shard_rows, head_width), jnp.float32),
    )


def finish(state, shard_rows):
    highest, weight_sum, weighted = state
    mixed_heads = weighted / weight_sum[:, :, None]
    joined = jnp.transpose(mixed_heads, (1, 0, 2))
    return joined.reshape(shard_rows, weighted.shape[0] * weighted.shape[2]).astype(jnp.bfloat16)


def body(
    residual,
    query_wide,
    key_wide,
    value_wide,
    query_narrow,
    key_narrow,
    value_narrow,
    gate_wide,
    gate_narrow,
    out_wide,
    out_narrow,
    norm_gain,
    routing,
    route_weight,
    gate_weight,
    up_weight,
    down_weight,
):
    shard_rows = query_wide.shape[0]
    half_rows = shard_rows // 2
    sp_place = lax.axis_index("sp")
    first_query = sp_place * shard_rows
    running_wide = jnp.cumsum(jax.nn.log_sigmoid(gate_wide), axis=0)
    running_narrow = jnp.cumsum(jax.nn.log_sigmoid(gate_narrow), axis=0)
    pieces_wide, pieces_narrow = (
        lax.all_gather(running_wide, "sp", axis=0, tiled=True),
        lax.all_gather(running_narrow, "sp", axis=0, tiled=True),
    )
    every_wide = globalize(pieces_wide, shard_rows)
    every_narrow = globalize(pieces_narrow, shard_rows)
    late_first = first_query + half_rows
    halves = []
    for place, part_wide, part_narrow in (
        (first_query, query_wide[:half_rows], query_narrow[:half_rows]),
        (late_first, query_wide[half_rows:], query_narrow[half_rows:]),
    ):
        halves.append(
            (
                place,
                part_wide,
                part_narrow,
                lax.dynamic_slice_in_dim(every_wide, place, half_rows, 0),
                lax.dynamic_slice_in_dim(every_narrow, place, half_rows, 0),
            )
        )

    def half_state():
        return (
            fresh_state(gate_wide.shape[1], half_rows, HW),
            fresh_state(gate_narrow.shape[1], half_rows, HN),
        )

    state = (half_state(), half_state())
    keys_wide = lax.all_gather(key_wide, "sp", axis=0, tiled=True)
    values_wide = lax.all_gather(value_wide, "sp", axis=0, tiled=True)
    keys_narrow = lax.all_gather(key_narrow, "sp", axis=0, tiled=True)
    values_narrow = lax.all_gather(value_narrow, "sp", axis=0, tiled=True)
    span_rows = keys_wide.shape[0]
    block_size = math.gcd(span_rows, 2048)

    def visit(carried, position):
        inside = position * block_size

        def take_block(source):
            return lax.dynamic_slice_in_dim(source, inside, block_size, 0)

        def take_decay(source):
            return lax.dynamic_slice_in_dim(source, inside, block_size, 0)

        block_kw = take_block(keys_wide)
        block_vw = take_block(values_wide)
        block_kn = take_block(keys_narrow)
        block_vn = take_block(values_narrow)
        block_dw = take_decay(every_wide)
        block_dn = take_decay(every_narrow)

        def one_half(current, half):
            place, part_wide, part_narrow, query_decay_wide, query_decay_narrow = half

            def work(inner):
                first = head_block(
                    inner[0],
                    part_wide,
                    query_decay_wide,
                    block_kw,
                    block_vw,
                    block_dw,
                    inside,
                    place,
                    HW,
                )
                second = head_block(
                    inner[1],
                    part_narrow,
                    query_decay_narrow,
                    block_kn,
                    block_vn,
                    block_dn,
                    inside,
                    place,
                    HN,
                )
                return (first, second)

            def skip(inner):
                return inner

            return lax.cond(inside <= place + half_rows - 1, work, skip, current)

        updated = (one_half(carried[0], halves[0]), one_half(carried[1], halves[1]))
        return (updated, None)

    state, _ = lax.scan(visit, state, jnp.arange(span_rows // block_size, dtype=jnp.int32))
    att_wide = jnp.concatenate(
        [finish(state[0][0], half_rows), finish(state[1][0], half_rows)], axis=0
    )
    att_narrow = jnp.concatenate(
        [finish(state[0][1], half_rows), finish(state[1][1], half_rows)], axis=0
    )
    own_rows = residual.shape[0]
    tp_place = lax.axis_index("tp")
    rows_wide = lax.dynamic_slice_in_dim(
        out_wide, tp_place * att_wide.shape[1], att_wide.shape[1], 0
    )
    rows_narrow = lax.dynamic_slice_in_dim(
        out_narrow, tp_place * att_narrow.shape[1], att_narrow.shape[1], 0
    )
    first = jnp.dot(att_wide, rows_wide, preferred_element_type=jnp.float32)
    second = jnp.dot(att_narrow, rows_narrow, preferred_element_type=jnp.float32)
    mixed = lax.psum_scatter(
        (first + second).astype(jnp.bfloat16), "tp", scatter_dimension=0, tiled=True
    ).astype(jnp.float32)
    middle = (residual.astype(jnp.float32) + mixed).astype(jnp.bfloat16)
    middle_wide = middle.astype(jnp.float32)
    spread = jnp.mean(middle_wide * middle_wide, axis=1, keepdims=True)
    normed = (middle_wide * lax.rsqrt(spread + epsilon) * norm_gain).astype(jnp.bfloat16)
    features = normed.shape[1]
    chosen_count = routing.shape[1]
    expert_count = gate_weight.shape[0] * lax.axis_size("sp")
    capacity = own_rows * GROUPS // expert_count
    flat_routes = routing.reshape(-1)
    matches = (flat_routes[:, None] == jnp.arange(expert_count, dtype=jnp.int32)[None, :]).astype(
        jnp.int32
    )
    ranking = jnp.sum((jnp.cumsum(matches, axis=0) - matches) * matches, axis=1)
    placing = flat_routes * capacity + ranking
    picker = (
        placing[None, :] == jnp.arange(expert_count * capacity, dtype=jnp.int32)[:, None]
    ).astype(jnp.bfloat16)
    picker = jnp.sum(picker.reshape(expert_count * capacity, own_rows, chosen_count), axis=2)
    outgoing = jnp.dot(picker, normed, preferred_element_type=jnp.float32).astype(jnp.bfloat16)
    outgoing = outgoing.reshape(expert_count, capacity, features)
    arrived = lax.all_to_all(outgoing, "sp", split_axis=0, concat_axis=0, tiled=True)
    pooled = lax.all_gather(arrived.reshape(-1, features), "tp", axis=0, tiled=True)
    gate_value = jnp.dot(pooled, gate_weight[0], preferred_element_type=jnp.float32)
    up_value = jnp.dot(pooled, up_weight[0], preferred_element_type=jnp.float32)
    hidden = (jax.nn.silu(gate_value) * up_value).astype(jnp.bfloat16)
    answers = lax.psum_scatter(
        jnp.dot(hidden, down_weight[0], preferred_element_type=jnp.float32).astype(jnp.bfloat16),
        "tp",
        scatter_dimension=0,
        tiled=True,
    )
    returned = lax.all_to_all(
        answers.reshape(expert_count, capacity, features),
        "sp",
        split_axis=0,
        concat_axis=0,
        tiled=True,
    )
    picked = jnp.take(returned.reshape(expert_count * capacity, features), placing, axis=0)
    picked = picked.reshape(own_rows, chosen_count, features).astype(jnp.float32)
    combined = jnp.sum(route_weight[:, :, None] * picked, axis=1)
    return (middle_wide + combined).astype(jnp.bfloat16)


def solution(mesh):
    placed = (
        P(("sp", "tp"), None),
        P("sp", "tp"),
        P("sp", "tp"),
        P("sp", "tp"),
        P("sp", "tp"),
        P("sp", "tp"),
        P("sp", "tp"),
        P("sp", "tp"),
        P("sp", "tp"),
        P(),
        P(),
        P(),
        P(("sp", "tp"), None),
        P(("sp", "tp"), None),
        P("sp", None, "tp"),
        P("sp", None, "tp"),
        P("sp", "tp", None),
    )
    return jax.shard_map(
        body, mesh=mesh, in_specs=placed, out_specs=P(("sp", "tp"), None), check_vma=False
    )
```

profile of v0, /device:TPU:0, one launch (start us, length us, event | category | flops | bytes accessed | tf_op | source)
XLA Modules:
  0.0 408.9 jit_solution(1248506105477989104)
XLA Ops:
  8.5 27.9 %all_gather.25 = f32[2048,2]{0,1:T(2,128)S(1)} all-gather(f32[256,2]{0,1:T(2,128)S(1)} %bitcast.168), channel_id=1, replica_groups=mesh['sp'=8,'tp'=4] {'sp'}, dimensions={0}, use_global_device_ids=true | all-gather | bytes 18432 | tf_op jit(solution)/shard_map/all_gather | solution.py:89
  38.3 19.0 %all_gather.22 = f32[2048,1]{0,1:T(1,128)S(1)} all-gather(f32[256,1]{0,1:T(1,128)S(1)} %reduce_window_sum.69), channel_id=1, replica_groups=mesh['sp'=8,'tp'=4] {'sp'}, dimensions={0}, use_global_device_ids=true | all-gather | bytes 9216 | tf_op jit(solution)/shard_map/all_gather | solution.py:88
  58.3 0.9 copy.47
  59.3 33.5 %all_gather.24 = bf16[2048,128]{0,1:T(8,128)(2,1)} all-gather(bf16[256,128]{0,1:T(8,128)(2,1)S(1)} %copy.47), channel_id=1, replica_groups=mesh['sp'=8,'tp'=4] {'sp'}, dimensions={0}, use_global_device_ids=true | all-gather | bytes 589824 | tf_op jit(solution)/shard_map/all_gather | solution.py:118
  92.8 0.9 copy.49
  93.7 31.4 %all_gather.26 = bf16[2048,128]{0,1:T(8,128)(2,1)S(1)} all-gather(bf16[256,128]{0,1:T(8,128)(2,1)S(1)} %copy.49), channel_id=1, replica_groups=mesh['sp'=8,'tp'=4] {'sp'}, dimensions={0}, use_global_device_ids=true | all-gather | bytes 589824 | tf_op jit(solution)/shard_map/all_gather | solution.py:119
  125.1 33.7 %all_gather.21 = bf16[2048,128]{1,0:T(8,128)(2,1)} all-gather(bf16[256,128]{1,0:T(8,128)(2,1)} %param.23), channel_id=1, replica_groups=mesh['sp'=8,'tp'=4] {'sp'}, dimensions={0}, use_global_device_ids=true | all-gather | bytes 589824 | tf_op jit(solution)/shard_map/all_gather | solution.py:116
  158.9 31.2 %all_gather.23 = bf16[2048,128]{1,0:T(8,128)(2,1)S(1)} all-gather(bf16[256,128]{1,0:T(8,128)(2,1)S(1)} %copy-done.5), channel_id=1, replica_groups=mesh['sp'=8,'tp'=4] {'sp'}, dimensions={0}, use_global_device_ids=true | all-gather | bytes 589824 | tf_op jit(solution)/shard_map/all_gather | solution.py:117
  192.3 10.5 %conditional.3 = (f32[1,128]{1,0:T(1,128)S(1)}, f32[1,128,128]{2,1,0:T(8,128)S(1)}, f32[2,128]{1,0:T(2,128)}, f32[2,128,64]{1,2,0:T(8,128)}) conditional(s32[]{:T(128)} %convert_element_type.106, (f32[1,128]{1,0:T(1,128)}, f32[1,128,128]{2,1,0:T(8,128)S(1)}, f32[2,128]{1,0:T(2,128)}, f32[2,128,64]{1,2,0:T(8,128)S(1)}) %tuple.35, (s32[]{:T(128)}, ...), branch_computations={%region_12.13_spmd, %region_13.18_spmd.clone} | conditional | flops 276104320 | bytes 15037726 | solution.py:170
  193.7 1.6 copy.51
  196.1 1.9 fusion.86
  198.4 1.3 multiply_add_fusion.1
  199.7 1.2 convolution_add_fusion.1
  203.3 8.7 %conditional.2 = ((f32[1,128]{1,0:T(1,128)}, f32[1,128,128]{2,1,0:T(8,128)S(1)}, f32[2,128]{1,0:T(2,128)}, f32[2,128,64]{1,2,0:T(8,128)S(1)})) conditional(s32[]{:T(128)} %convert_element_type.103, (f32[1,128]{1,0:T(1,128)}, f32[1,128,128]{2,1,0:T(8,128)S(1)}, f32[2,128]{1,0:T(2,128)}, f32[2,128,64]{1,2,0:T(8,128)S(1)}) %tuple.35, (s32[]{:T(128)}, ...), branch_computations={%region_6.7_spmd, %region_7.12_spmd.clone} | conditional | flops 276104320 | bytes 15033570 | solution.py:170
  204.3 0.9 copy.50
  205.2 1.9 fusion.84
  207.7 1.3 multiply_add_fusion
  210.8 1.2 bitcast_add_fusion
  214.7 2.5 fusion.38
  218.3 21.2 %reduce-scatter.3.cloned.1.call-done = bf16[64,2048]{1,0:T(8,128)(2,1)} async-done(((bf16[256,2048]{1,0:T(8,128)(2,1)}), bf16[64,2048]{1,0:T(8,128)(2,1)}) %reduce-scatter.3.cloned.1.call-update) | async-done | bytes 262160 | tf_op jit(solution)/shard_map/reduce_scatter | solution.py:192
  239.5 1.1 fusion.50
  240.7 1.4 convolution_convert_fusion.1
  242.2 31.1 %all_to_all.10 = bf16[8,32,2048]{2,1,0:T(8,128)(2,1)} all-to-all(bf16[8,32,2048]{2,1,0:T(8,128)(2,1)S(1)} %bitcast.150), channel_id=1, replica_groups=mesh['sp'=8,'tp'=4] {'sp'}, dimensions={0} | all-to-all | bytes 2097152 | tf_op jit(solution)/shard_map/all_to_all | solution.py:215
  273.6 32.5 %all-gather.2.cloned.1.call-done = bf16[1024,2048]{1,0:T(8,128)(2,1)} async-done(((bf16[256,2048]{1,0:T(8,128)(2,1)}), bf16[1024,2048]{1,0:T(8,128)(2,1)}) %all-gather.2.cloned.1.call-update) | async-done | bytes 4194320 | tf_op jit(solution)/shard_map/all_gather | solution.py:216
  306.0 4.5 %fusion.43 = f32[1024,256]{1,0:T(8,128)} fusion(bf16[1024,2048]{1,0:T(8,128)(2,1)} %all-gather.2.cloned.1.call-done, bf16[1,2048,256]{2,1,0:T(8,128)(2,1)S(1)} %copy-done.18), kind=kOutput, calls=%fused_computation.73 | convolution fusion | flops 1073741824 | bytes 6291456 | tf_op jit(solution)/shard_map/dot_general | solution.py:217
  310.5 9.4 %convolution_convert_fusion = bf16[1024,2048]{1,0:T(8,128)(2,1)} fusion(bf16[1024,2048]{1,0:T(8,128)(2,1)} %all-gather.2.cloned.1.call-done, bf16[1,256,2048]{2,1,0:T(8,128)(2,1)} %param.37, bf16[1,2048,256]{2,1,0:T(8,128)(2,1)} %param.36, f32[1024,256]{1,0:T(8,128)} %fusion.43), kind=kOutput, calls=%fused_computation.65 | convolution fusion | flops 2151153664 | bytes 11534336 | tf_op jit(solution)/shard_map/dot_general | solution.py:221
  320.0 44.7 %reduce-scatter.5.cloned.1.call-done = bf16[256,2048]{1,0:T(8,128)(2,1)} async-done(((bf16[1024,2048]{1,0:T(8,128)(2,1)}), bf16[256,2048]{1,0:T(8,128)(2,1)}) %reduce-scatter.5.cloned.1.call-update) | async-done | bytes 1048592 | tf_op jit(solution)/shard_map/reduce_scatter | solution.py:220
  364.7 5.5 %all-to-all-start.1 = ((bf16[8,32,2048]{2,1,0:T(8,128)(2,1)}), bf16[8,32,2048]{2,1,0:T(8,128)(2,1)S(1)}, u32[]{:S(2)}, u32[]{:S(2)}) async-start(bf16[8,32,2048]{2,1,0:T(8,128)(2,1)} %bitcast.151), calls=%async_computation.3 | async-start | bytes 2097152 | tf_op jit(solution)/shard_map/all_to_all | solution.py:226
  370.7 25.2 %all-to-all-done.1 = bf16[8,32,2048]{2,1,0:T(8,128)(2,1)S(1)} async-done(((bf16[8,32,2048]{2,1,0:T(8,128)(2,1)}), bf16[8,32,2048]{2,1,0:T(8,128)(2,1)S(1)}, u32[]{:S(2)}, u32[]{:S(2)}) %all-to-all-start.1) | async-done | bytes 1048608 | tf_op jit(solution)/shard_map/all_to_all | solution.py:226
  395.9 1.7 gather_fusion
  397.6 1.4 gather.7
  399.0 2.5 multiply_reduce_fusion
  (130 shorter events, 20.7 us)
Async XLA Ops:
  6.5 207.7 %copy-start = (bf16[512,2048]{1,0:T(8,128)(2,1)S(1)}, bf16[512,2048]{1,0:T(8,128)(2,1)}, u32[]{:S(2)}) copy-start(bf16[512,2048]{1,0:T(8,128)(2,1)} %param.30) | copy-start | bytes 6291460
  6.5 152.3 %copy-start.5 = (bf16[256,128]{1,0:T(8,128)(2,1)S(1)}, bf16[256,128]{1,0:T(8,128)(2,1)}, u32[]{:S(2)}) copy-start(bf16[256,128]{1,0:T(8,128)(2,1)} %param.24) | copy-start | bytes 196612
  6.5 233.0 %reduce-scatter.3.cloned.1.call-start = ((), (), s32[]{:S(2)}) async-start(), calls=%async_computation.4 | async-start | bytes 1310720 | tf_op jit(solution)/shard_map/reduce_scatter | solution.py:192
  192.9 0.6 copy-start.15
  195.3 2.6 copy-start.6
  198.0 2.9 copy-start.10
  198.0 3.0 copy-start.3
  198.0 3.0 copy-start.16
  198.0 3.0 copy-start.19
  199.7 1.8 copy-start.12
  202.8 0.5 copy-start.17
  203.4 3.8 copy-start.7
  207.2 2.3 copy-start.11
  207.2 2.4 copy-start.4
  207.2 2.4 copy-start.20
  208.9 1.2 copy-start.13
  214.7 2.7 copy-start.8
  214.7 24.9 %copy-start.1 = (bf16[64,2048]{1,0:T(8,128)(2,1)S(1)}, bf16[64,2048]{1,0:T(8,128)(2,1)}, u32[]{:S(2)}) copy-start(bf16[64,2048]{1,0:T(8,128)(2,1)} %param.21) | copy-start | bytes 786436
  214.7 26.0 %copy-start.9 = (f32[2048]{0:T(1024)S(1)}, f32[2048]{0:T(1024)}, u32[]{:S(2)}) copy-start(f32[2048]{0:T(1024)} %param.32) | copy-start | bytes 24580
  217.3 88.8 %all-gather.2.cloned.1.call-start = ((), (), s32[]{:S(2)}) async-start(), calls=%async_computation.5 | async-start | bytes 5242880 | tf_op jit(solution)/shard_map/all_gather | solution.py:216
  242.1 63.9 %copy-start.18 = (bf16[1,2048,256]{2,1,0:T(8,128)(2,1)S(1)}, bf16[1,2048,256]{2,1,0:T(8,128)(2,1)}, u32[]{:S(2)}) copy-start(bf16[1,2048,256]{2,1,0:T(8,128)(2,1)} %param.35) | copy-start | bytes 3145732
  273.3 91.4 %reduce-scatter.5.cloned.1.call-start = ((), (), s32[]{:S(2)}) async-start(), calls=%async_computation.6 | async-start | bytes 5242880 | tf_op jit(solution)/shard_map/reduce_scatter | solution.py:220
  320.0 50.6 %copy-start.14 = (f32[64,2]{0,1:T(2,128)S(1)}, f32[64,2]{0,1:T(2,128)}, u32[]{:S(2)}) copy-start(f32[64,2]{0,1:T(2,128)} %param.34) | copy-start | bytes 1540
  364.7 31.2 %all-to-all-start.1 = ((bf16[8,32,2048]{2,1,0:T(8,128)(2,1)}), bf16[8,32,2048]{2,1,0:T(8,128)(2,1)S(1)}, u32[]{:S(2)}, u32[]{:S(2)}) async-start(bf16[8,32,2048]{2,1,0:T(8,128)(2,1)} %bitcast.151), calls=%async_computation.3 | async-start | bytes 2097152 | tf_op jit(solution)/shard_map/all_to_all | solution.py:226
  397.6 4.0 copy-start.2
Sparse Core Ops, SparseCore 0:
  217.4 22.1 reduce-scatter.2
  273.5 32.5 all-gather.1
  320.1 44.5 reduce-scatter.4
where the time goes:
time: 410 us; the launch traced here: 409 us
  blocking collectives  208 us (51%)
  waiting for transfers between devices  124 us (30%)
  matrix products  25.6 us (6%)
  other arithmetic  18.2 us (4%)
  local copies, waits for them, and re-layouts  14.4 us (4%)
  between operations  13.4 us (3%)
  starting transfers between devices  5.77 us (1%)
    reduce_scatter x1, waiting for transfers between devices, body(): lax.psum_scatter(jnp.dot(hidden, down_weight[0], preferred_element_type=j...  44.7 us
    all_gather x1, blocking collectives, body(): keys_wide = lax.all_gather(key_wide, 'sp', axis=0, tiled=True)  33.7 us
    all_gather x1, blocking collectives, body(): keys_narrow = lax.all_gather(key_narrow, 'sp', axis=0, tiled=True)  33.5 us
    all_gather x1, waiting for transfers between devices, body(): lax.all_gather(arrived.reshape(-1, features), 'tp', axis=0, tiled=True)  32.5 us
    all_gather x1, blocking collectives, body(): values_narrow = lax.all_gather(value_narrow, 'sp', axis=0, tiled=True)  31.4 us
    all_gather x1, blocking collectives, body(): values_wide = lax.all_gather(value_wide, 'sp', axis=0, tiled=True)  31.2 us
    all_to_all x1, blocking collectives, body(): lax.all_to_all(outgoing, 'sp', split_axis=0, concat_axis=0, tiled=True)  31.1 us
    all_gather x1, blocking collectives, body(): lax.all_gather(running_narrow, 'sp', axis=0, tiled=True)  27.9 us
  transfers between devices with their start and end apart: 4, of which 4 were waited for; matrix products, arithmetic and copies ran while one was open for 0% of the time, Pallas kernels for 0%

commit v1 on v0

--- a/solution.py
+++ b/solution.py
@@ -114,8 +114,11 @@
 
     state = (half_state(), half_state())
     keys_wide = lax.all_gather(key_wide, "sp", axis=0, tiled=True)
-    values_wide = lax.all_gather(value_wide, "sp", axis=0, tiled=True)
-    keys_narrow = lax.all_gather(key_narrow, "sp", axis=0, tiled=True)
+    values_wide, keys_narrow = jnp.split(
+        lax.all_gather(jnp.concatenate([value_wide, key_narrow], axis=1), "sp", axis=0, tiled=True),
+        [value_wide.shape[1]],
+        axis=1,
+    )
     values_narrow = lax.all_gather(value_narrow, "sp", axis=0, tiled=True)
     span_rows = keys_wide.shape[0]
     block_size = math.gcd(span_rows, 2048)

time: 410 us -> 349 us (0.85)
  blocking collectives: 208 us -> 143 us
    all_gather x2 -> x0, blocking collectives: 64.7 us -> none  [the longest x1 33.5 us: body(): keys_narrow = lax.all_gather(key_narrow, 'sp', axis=0, tiled=True)]
  transfers between devices with their start and end apart: 4 -> 5, of which waited for: 4 -> 4; matrix products, arithmetic and copies ran while one was open for 0% -> 2% of each run, Pallas kernels for 0% -> 0%
where the time goes in v1:
time: 349 us; the launch traced here: 348 us
  blocking collectives  143 us (41%)
  waiting for transfers between devices  124 us (36%)
  matrix products  25.6 us (7%)
  other arithmetic  18.8 us (5%)
  local copies, waits for them, and re-layouts  17.7 us (5%)
  between operations  13.4 us (4%)
  starting transfers between devices  5.82 us (2%)
    reduce_scatter x1, waiting for transfers between devices, body(): lax.psum_scatter(jnp.dot(hidden, down_weight[0], preferred_element_type=j...  44.7 us
    all_gather x1, blocking collectives, body(): keys_wide = lax.all_gather(key_wide, 'sp', axis=0, tiled=True)  33.5 us
    all_gather x1, waiting for transfers between devices, body(): lax.all_gather(arrived.reshape(-1, features), 'tp', axis=0, tiled=True)  32.5 us
    all_gather x1, blocking collectives, body(): values_narrow = lax.all_gather(value_narrow, 'sp', axis=0, tiled=True)  31.5 us
    all_to_all x1, blocking collectives, body(): lax.all_to_all(outgoing, 'sp', split_axis=0, concat_axis=0, tiled=True)  31.1 us
    all_gather x1, blocking collectives, body(): lax.all_gather(running_narrow, 'sp', axis=0, tiled=True)  28 us
    all_to_all x1, waiting for transfers between devices, body(): lax.all_to_all(answers.reshape(expert_count, capacity, features), 'sp', s...  25.2 us
    reduce_scatter x1, waiting for transfers between devices, body(): lax.psum_scatter((first + second).astype(jnp.bfloat16), 'tp', scatter_dim...  21.2 us
  transfers between devices with their start and end apart: 5, of which 4 were waited for; matrix products, arithmetic and copies ran while one was open for 2% of the time, Pallas kernels for 0%

profile of v1, /device:TPU:0, one launch (start us, length us, event | category | flops | bytes accessed | tf_op | source)
XLA Modules:
  0.0 348.2 jit_solution(2062480744564855352)
XLA Ops:
  6.5 1.1 copy.56
  7.6 0.9 copy.57
  11.1 28.0 %all_gather.21 = f32[2048,2]{0,1:T(2,128)S(1)} all-gather(f32[256,2]{0,1:T(2,128)S(1)} %bitcast.168), channel_id=1, replica_groups=mesh['sp'=8,'tp'=4] {'sp'}, dimensions={0}, use_global_device_ids=true | all-gather | bytes 18432 | tf_op jit(solution)/shard_map/all_gather | solution.py:89
  41.0 19.1 %all_gather.19 = f32[2048,1]{0,1:T(1,128)S(1)} all-gather(f32[256,1]{0,1:T(1,128)S(1)} %reduce_window_sum.69), channel_id=1, replica_groups=mesh['sp'=8,'tp'=4] {'sp'}, dimensions={0}, use_global_device_ids=true | all-gather | bytes 9216 | tf_op jit(solution)/shard_map/all_gather | solution.py:88
  61.1 0.9 copy.59
  63.2 31.5 %all_gather.22 = bf16[2048,128]{0,1:T(8,128)(2,1)S(1)} all-gather(bf16[256,128]{0,1:T(8,128)(2,1)S(1)} %copy.59), channel_id=1, replica_groups=mesh['sp'=8,'tp'=4] {'sp'}, dimensions={0}, use_global_device_ids=true | all-gather | bytes 589824 | tf_op jit(solution)/shard_map/all_gather | solution.py:122
  94.8 33.5 %all_gather.18 = bf16[2048,128]{1,0:T(8,128)(2,1)} all-gather(bf16[256,128]{1,0:T(8,128)(2,1)} %param.23), channel_id=1, replica_groups=mesh['sp'=8,'tp'=4] {'sp'}, dimensions={0}, use_global_device_ids=true | all-gather | bytes 589824 | tf_op jit(solution)/shard_map/all_gather | solution.py:116
  128.2 2.1 fusion.87
  131.4 10.5 %conditional.3 = (f32[1,128]{1,0:T(1,128)S(1)}, f32[1,128,128]{2,1,0:T(8,128)S(1)}, f32[2,128]{1,0:T(2,128)}, f32[2,128,64]{1,2,0:T(8,128)}) conditional(s32[]{:T(128)} %convert_element_type.106, (f32[1,128]{1,0:T(1,128)}, f32[1,128,128]{2,1,0:T(8,128)S(1)}, f32[2,128]{1,0:T(2,128)}, f32[2,128,64]{1,2,0:T(8,128)S(1)}) %tuple.35, (s32[]{:T(128)}, ...), branch_computations={%region_12.13_spmd, %region_13.18_spmd.clone} | conditional | flops 276104320 | bytes 15037726 | solution.py:173
  132.9 1.6 copy.63
  135.2 1.9 fusion.86
  137.6 1.2 multiply_add_fusion.1
  138.8 1.2 convolution_add_fusion.1
  142.5 8.7 %conditional.2 = ((f32[1,128]{1,0:T(1,128)}, f32[1,128,128]{2,1,0:T(8,128)S(1)}, f32[2,128]{1,0:T(2,128)}, f32[2,128,64]{1,2,0:T(8,128)S(1)})) conditional(s32[]{:T(128)} %convert_element_type.103, (f32[1,128]{1,0:T(1,128)}, f32[1,128,128]{2,1,0:T(8,128)S(1)}, f32[2,128]{1,0:T(2,128)}, f32[2,128,64]{1,2,0:T(8,128)S(1)}) %tuple.35, (s32[]{:T(128)}, ...), branch_computations={%region_6.7_spmd, %region_7.12_spmd.clone} | conditional | flops 276104320 | bytes 15033570 | solution.py:173
  143.5 0.9 copy.61
  144.5 1.9 fusion.84
  146.9 1.3 multiply_add_fusion
  150.0 1.2 bitcast_add_fusion
  154.1 2.5 fusion.38
  157.7 21.2 %reduce-scatter.3.cloned.1.call-done = bf16[64,2048]{1,0:T(8,128)(2,1)} async-done(((bf16[256,2048]{1,0:T(8,128)(2,1)}), bf16[64,2048]{1,0:T(8,128)(2,1)}) %reduce-scatter.3.cloned.1.call-update) | async-done | bytes 262160 | tf_op jit(solution)/shard_map/reduce_scatter | solution.py:195
  178.9 1.1 fusion.50
  180.0 1.4 convolution_convert_fusion.1
  181.5 31.1 %all_to_all.10 = bf16[8,32,2048]{2,1,0:T(8,128)(2,1)} all-to-all(bf16[8,32,2048]{2,1,0:T(8,128)(2,1)S(1)} %bitcast.150), channel_id=1, replica_groups=mesh['sp'=8,'tp'=4] {'sp'}, dimensions={0} | all-to-all | bytes 2097152 | tf_op jit(solution)/shard_map/all_to_all | solution.py:218
  212.9 32.5 %all-gather.5.cloned.1.call-done = bf16[1024,2048]{1,0:T(8,128)(2,1)} async-done(((bf16[256,2048]{1,0:T(8,128)(2,1)}), bf16[1024,2048]{1,0:T(8,128)(2,1)}) %all-gather.5.cloned.1.call-update) | async-done | bytes 4194320 | tf_op jit(solution)/shard_map/all_gather | solution.py:219
  245.3 4.5 %fusion.43 = f32[1024,256]{1,0:T(8,128)} fusion(bf16[1024,2048]{1,0:T(8,128)(2,1)} %all-gather.5.cloned.1.call-done, bf16[1,2048,256]{2,1,0:T(8,128)(2,1)S(1)} %copy-done.17), kind=kOutput, calls=%fused_computation.73 | convolution fusion | flops 1073741824 | bytes 6291456 | tf_op jit(solution)/shard_map/dot_general | solution.py:220
  249.8 9.4 %convolution_convert_fusion = bf16[1024,2048]{1,0:T(8,128)(2,1)} fusion(bf16[1024,2048]{1,0:T(8,128)(2,1)} %all-gather.5.cloned.1.call-done, bf16[1,256,2048]{2,1,0:T(8,128)(2,1)} %param.37, bf16[1,2048,256]{2,1,0:T(8,128)(2,1)} %param.36, f32[1024,256]{1,0:T(8,128)} %fusion.43), kind=kOutput, calls=%fused_computation.65 | convolution fusion | flops 2151153664 | bytes 11534336 | tf_op jit(solution)/shard_map/dot_general | solution.py:224
  259.3 44.7 %reduce-scatter.5.cloned.1.call-done = bf16[256,2048]{1,0:T(8,128)(2,1)} async-done(((bf16[1024,2048]{1,0:T(8,128)(2,1)}), bf16[256,2048]{1,0:T(8,128)(2,1)}) %reduce-scatter.5.cloned.1.call-update) | async-done | bytes 1048592 | tf_op jit(solution)/shard_map/reduce_scatter | solution.py:223
  304.0 5.5 %all-to-all-start.1 = ((bf16[8,32,2048]{2,1,0:T(8,128)(2,1)}), bf16[8,32,2048]{2,1,0:T(8,128)(2,1)S(1)}, u32[]{:S(2)}, u32[]{:S(2)}) async-start(bf16[8,32,2048]{2,1,0:T(8,128)(2,1)} %bitcast.151), calls=%async_computation.3 | async-start | bytes 2097152 | tf_op jit(solution)/shard_map/all_to_all | solution.py:229
  310.0 25.2 %all-to-all-done.1 = bf16[8,32,2048]{2,1,0:T(8,128)(2,1)S(1)} async-done(((bf16[8,32,2048]{2,1,0:T(8,128)(2,1)}), bf16[8,32,2048]{2,1,0:T(8,128)(2,1)S(1)}, u32[]{:S(2)}, u32[]{:S(2)}) %all-to-all-start.1) | async-done | bytes 1048608 | tf_op jit(solution)/shard_map/all_to_all | solution.py:229
  335.2 1.7 gather_fusion
  336.9 1.4 gather.7
  338.3 2.5 multiply_reduce_fusion
  (132 shorter events, 21.4 us)
Async XLA Ops:
  6.5 147.0 %copy-start = (bf16[512,2048]{1,0:T(8,128)(2,1)S(1)}, bf16[512,2048]{1,0:T(8,128)(2,1)}, u32[]{:S(2)}) copy-start(bf16[512,2048]{1,0:T(8,128)(2,1)} %param.30) | copy-start | bytes 6291460
  6.5 121.7 %all-gather.3.cloned.1.call-start = ((), (), s32[]{:S(2)}) async-start(), calls=%async_computation.4 | async-start | bytes 1179648 | tf_op jit(solution)/shard_map/all_gather | solution.py:118
  9.3 169.6 %reduce-scatter.3.cloned.1.call-start = ((), (), s32[]{:S(2)}) async-start(), calls=%async_computation.5 | async-start | bytes 1310720 | tf_op jit(solution)/shard_map/reduce_scatter | solution.py:195
  132.1 0.6 copy-start.14
  134.4 2.6 copy-start.5
  137.1 2.9 copy-start.9
  137.1 3.0 copy-start.3
  137.1 3.0 copy-start.15
  137.1 3.0 copy-start.18
  138.8 1.8 copy-start.11
  141.9 0.6 copy-start.16
  142.6 3.8 %copy-start.6 = (f32[2,128]{1,0:T(2,128)S(1)}, f32[2,128]{1,0:T(2,128)}, u32[]{:S(2)}) copy-start(f32[2,128]{1,0:T(2,128)} %get-tuple-element.417) | copy-start | bytes 3076 | tf_op jit(solution)/shard_map/while/body/eval_jaxpr/cond
  146.4 2.3 copy-start.10
  146.4 2.4 copy-start.4
  146.4 2.4 copy-start.19
  148.1 1.2 copy-start.12
  154.0 2.7 copy-start.7
  154.0 24.8 %copy-start.1 = (bf16[64,2048]{1,0:T(8,128)(2,1)S(1)}, bf16[64,2048]{1,0:T(8,128)(2,1)}, u32[]{:S(2)}) copy-start(bf16[64,2048]{1,0:T(8,128)(2,1)} %param.21) | copy-start | bytes 786436
  154.0 26.0 %copy-start.8 = (f32[2048]{0:T(1024)S(1)}, f32[2048]{0:T(1024)}, u32[]{:S(2)}) copy-start(f32[2048]{0:T(1024)} %param.32) | copy-start | bytes 24580
  156.6 88.7 %all-gather.5.cloned.1.call-start = ((), (), s32[]{:S(2)}) async-start(), calls=%async_computation.6 | async-start | bytes 5242880 | tf_op jit(solution)/shard_map/all_gather | solution.py:219
  181.5 63.9 %copy-start.17 = (bf16[1,2048,256]{2,1,0:T(8,128)(2,1)S(1)}, bf16[1,2048,256]{2,1,0:T(8,128)(2,1)}, u32[]{:S(2)}) copy-start(bf16[1,2048,256]{2,1,0:T(8,128)(2,1)} %param.35) | copy-start | bytes 3145732
  212.6 91.4 %reduce-scatter.5.cloned.1.call-start = ((), (), s32[]{:S(2)}) async-start(), calls=%async_computation.7 | async-start | bytes 5242880 | tf_op jit(solution)/shard_map/reduce_scatter | solution.py:223
  259.3 50.6 %copy-start.13 = (f32[64,2]{0,1:T(2,128)S(1)}, f32[64,2]{0,1:T(2,128)}, u32[]{:S(2)}) copy-start(f32[64,2]{0,1:T(2,128)} %param.34) | copy-start | bytes 1540
  304.0 31.2 %all-to-all-start.1 = ((bf16[8,32,2048]{2,1,0:T(8,128)(2,1)}), bf16[8,32,2048]{2,1,0:T(8,128)(2,1)S(1)}, u32[]{:S(2)}, u32[]{:S(2)}) async-start(bf16[8,32,2048]{2,1,0:T(8,128)(2,1)} %bitcast.151), calls=%async_computation.3 | async-start | bytes 2097152 | tf_op jit(solution)/shard_map/all_to_all | solution.py:229
  336.9 4.0 %copy-start.2 = (bf16[64,2048]{1,0:T(8,128)(2,1)S(1)}, bf16[64,2048]{1,0:T(8,128)(2,1)}, u32[]{:S(2)}) copy-start(bf16[64,2048]{1,0:T(8,128)(2,1)} %reduce-scatter.3.cloned.1.call-done) | copy-start | bytes 786436
Sparse Core Ops, SparseCore 0:
  9.4 42.1 all-gather.2
  156.7 22.0 reduce-scatter.2
  212.8 32.5 all-gather.4
  259.4 44.5 reduce-scatter.4
